TPU v7x, 256 devices: a whole 4x4x8 slice. The times are simulated.
256 devices in a mesh: ep: 64 (over z, y, core), tp: 4 (over x).
Axes of the slice: x: 4, y: 4, z: 8, core: 2. Of those that a mesh axis runs over, the one named last changes fastest.
Arguments:
- queries: bfloat16 [16384, 8, 128], P('ep', 'tp'), may hold values from -15 to 15
- keys: bfloat16 [16384, 4, 128], P('ep', 'tp'), may hold values from -6 to 6
- values: bfloat16 [16384, 4, 128], P('ep', 'tp'), may hold values from -6 to 6
- key_bias: bfloat16 [16384, 8], P('ep', 'tp'), may hold values from -20 to 2
- out_weight: bfloat16 [1024, 2048], P('tp'), may hold values from -0.1875 to 0.1875
- tokens_b: bfloat16 [32768, 2048], P(('ep', 'tp')), may hold values from -6 to 6
- moe_gain: bfloat16 [2048], replicated, may hold values from 0.099609375 to 1.8984375
- gate_weight: bfloat16 [64, 2048, 2048], P('ep', None, 'tp'), may hold values from -0.125 to 0.125
- up_weight: bfloat16 [64, 2048, 2048], P('ep', None, 'tp'), may hold values from -0.125 to 0.125
- down_weight: bfloat16 [64, 2048, 2048], P('ep', 'tp'), may hold values from -0.125 to 0.125
- routes: int32 [32768, 2], P(('ep', 'tp')), may hold values from 0 to 63, all different within a row; in each aligned block of 128 rows (0 to 127, 128 to 255, ...) at most 6 rows name the same one
- route_weights: float32 [32768, 2], P(('ep', 'tp')), may hold values from 0.2 to 1
Outputs:
- mixed: bfloat16 [16384, 2048], P(('ep', 'tp'))
- moe_out: bfloat16 [32768, 2048], P(('ep', 'tp'))
Inputs may be any that keep to these rules, and one draw needn't show every extreme that they name: `routes`: each row names 2 different experts. In each aligned block of 128 rows (the rows of one device) no expert is named by more than 6 rows, and in some block one expert is named by exactly 6 rows.
All inputs are finite; a program needn't handle non-finite values.
Results may differ from a plain program's by a relative error of at most 0.012.
Values may be sent and summed in bfloat16 or wider, within the bound.
A program may use at most 128 MiB of HBM per device.

v0:
```python
import math
import jax
import jax.numpy as jnp
from jax import lax
from jax.sharding import PartitionSpec as P


def in_one_piece(arrays, axis, dim, along):
    columns = [a.reshape(*a.shape[:along], -1) for a in arrays]
    both = jnp.concatenate(columns, axis=along)
    filled, at, done = (lax.all_gather(both, axis, axis=dim, tiled=True), 0, [])
    for a, column in zip(arrays, columns):
        share = filled[..., at : at + column.shape[along]]
        done.append(share.reshape(*share.shape[:along], *a.shape[along:]))
        at += column.shape[along]
    return tuple(done)


def partner(value, axis, apart):
    mask = 2**apart
    pairs = [(source, source ^ mask) for source in range(lax.axis_size(axis))]
    return lax.ppermute(value, axis, pairs)


def split_up(value, dim, length):
    before, after = (value.shape[:dim], value.shape[dim + 1 :])
    return jnp.moveaxis(value.reshape(*before, length, -1, *after), dim, 0)


def summed_on_arrival(value, axis, dim):
    pieces = split_up(value, dim, lax.axis_size(axis))
    arrived = lax.all_to_all(pieces, axis, split_axis=0, concat_axis=0, tiled=True)
    return arrived.astype(jnp.float32).sum(axis=0)


def entry_slots(routes, expert_total):
    flattened_expert_list = routes.reshape(-1)
    onehot = (
        flattened_expert_list[:, None] == jnp.arange(expert_total, dtype=jnp.int32)[None, :]
    ).astype(jnp.int32)
    earlier_count = jnp.cumsum(onehot, axis=0) - onehot
    return (flattened_expert_list, jnp.sum(earlier_count * onehot, axis=1))


def swiglu_rows(piece, gate_cols, up_cols):
    gate_val = jnp.dot(piece, gate_cols, preferred_element_type=jnp.float32)
    up_val = jnp.dot(piece, up_cols, preferred_element_type=jnp.float32)
    return (jax.nn.silu(gate_val) * up_val).astype(jnp.bfloat16)


def attend_rows(query_block, first_pos, keys_all, values_all, bias_all, local_kv):
    row_count, local_heads, head_dim = query_block.shape
    group_size = local_heads // local_kv
    key_total = keys_all.shape[0]
    key_span = min(1024, key_total)
    query_pos = first_pos + jnp.arange(row_count, dtype=jnp.int32)
    query_rows = query_block.reshape(row_count, local_kv, group_size, head_dim)
    visit_total = (first_pos + row_count + key_span - 1) // key_span
    score_scale = 1.0 / math.sqrt(head_dim)

    def visit(visit_no, state):
        accum, carried = state
        begin_at = (visit_total - 1 - visit_no) * key_span
        key_tile_rows = lax.dynamic_slice_in_dim(keys_all, begin_at, key_span, 0)
        value_block = lax.dynamic_slice_in_dim(values_all, begin_at, key_span, 0)
        bias_block = (
            lax.dynamic_slice_in_dim(bias_all, begin_at, key_span, 0)
            .astype(jnp.float32)
            .reshape(key_span, local_kv, group_size)
        )
        scores = (
            jnp.einsum(
                "rkgd,skd->kgrs", query_rows, key_tile_rows, preferred_element_type=jnp.float32
            )
            * score_scale
        )
        scores = scores + jnp.transpose(bias_block, (1, 2, 0))[:, :, None, :]
        key_pos = begin_at + jnp.arange(key_span, dtype=jnp.int32)
        earlier = key_pos[None, :] < query_pos[:, None]
        log_keep = jnp.where(earlier, jax.nn.log_sigmoid(-scores), 0.0)
        after = lax.cumsum(log_keep, axis=3, reverse=True) - log_keep
        weights = jnp.where(
            earlier, jnp.exp(jax.nn.log_sigmoid(scores) + after + carried[..., None]), 0.0
        ).astype(jnp.bfloat16)
        accum = accum + jnp.einsum(
            "kgrs,skd->kgrd", weights, value_block, preferred_element_type=jnp.float32
        )
        return (accum, carried + jnp.sum(log_keep, axis=3))

    start_state = (
        jnp.zeros((local_kv, group_size, row_count, head_dim), jnp.float32),
        jnp.zeros((local_kv, group_size, row_count), jnp.float32),
    )
    accum = lax.fori_loop(0, visit_total, visit, start_state)[0]
    return (
        jnp.transpose(accum, (2, 0, 1, 3))
        .reshape(row_count, local_heads * head_dim)
        .astype(jnp.bfloat16)
    )


def body(
    queries,
    keys,
    values,
    key_bias,
    out_weight,
    tokens_b,
    moe_gain,
    gate_weight,
    up_weight,
    down_weight,
    routes,
    route_weights,
):
    tok_rows, local_heads, head_dim = queries.shape
    local_kv = keys.shape[1]
    ep_count = lax.axis_size("ep")
    keys_all, values_all, bias_all = in_one_piece((keys, values, key_bias), "ep", 0, 1)
    device_ep = lax.axis_index("ep")
    half_rows = tok_rows // 2
    bit_count = ep_count.bit_length() - 1
    handed = queries[half_rows:]
    for bit_no in range(bit_count):
        handed = partner(handed, "ep", bit_no)
    companion_batch = ep_count - 1 - device_ep
    own_part = attend_rows(
        queries[:half_rows], device_ep * tok_rows, keys_all, values_all, bias_all, local_kv
    )
    other_part = attend_rows(
        handed, companion_batch * tok_rows + half_rows, keys_all, values_all, bias_all, local_kv
    )
    for bit_no in range(bit_count):
        other_part = partner(other_part, "ep", bit_no)
    attended = jnp.concatenate((own_part, other_part), axis=0)
    tok_b, model_width = tokens_b.shape
    top_count = routes.shape[1]
    expert_total = ep_count * gate_weight.shape[0]
    capacity = max(2, 3 * top_count * tok_b // (2 * expert_total))
    tokens_f = tokens_b.astype(jnp.float32)
    normed = (
        tokens_f
        * lax.rsqrt(jnp.mean(tokens_f * tokens_f, axis=1, keepdims=True) + 1e-06)
        * moe_gain.astype(jnp.float32)
    ).astype(jnp.bfloat16)
    flattened_expert_list, slot_index = entry_slots(routes, expert_total)
    place = flattened_expert_list * capacity + slot_index
    outbound = (
        jnp.zeros((expert_total * capacity, model_width), jnp.bfloat16)
        .at[place]
        .set(jnp.repeat(normed, top_count, axis=0))
    )
    outbound = outbound.reshape(expert_total, capacity, model_width)
    gate_cols = gate_weight[0]
    up_cols = up_weight[0]
    down_rows = down_weight[0]
    arrived = lax.all_to_all(outbound, "ep", split_axis=0, concat_axis=0, tiled=True)
    hidden = swiglu_rows(
        lax.all_gather(arrived.reshape(ep_count * capacity, model_width), "tp", axis=0, tiled=True),
        gate_cols,
        up_cols,
    )
    mixed_sum = lax.psum_scatter(
        jnp.dot(attended, out_weight, preferred_element_type=jnp.float32).astype(jnp.bfloat16),
        "tp",
        scatter_dimension=0,
        tiled=True,
    )
    expert_sum = summed_on_arrival(
        jnp.dot(hidden, down_rows, preferred_element_type=jnp.float32).astype(jnp.bfloat16), "tp", 0
    )
    returned = lax.all_to_all(
        expert_sum.astype(jnp.bfloat16).reshape(ep_count, capacity, model_width),
        "ep",
        split_axis=0,
        concat_axis=0,
        tiled=True,
    )
    picked = jnp.take(returned.reshape(expert_total * capacity, model_width), place, axis=0).astype(
        jnp.float32
    )
    weighted = picked * route_weights.reshape(-1)[:, None]
    moe_out = jnp.sum(weighted.reshape(tok_b, top_count, model_width), axis=1).astype(jnp.bfloat16)
    return (mixed_sum, moe_out)


def solution(mesh):
    in_specs = (
        P("ep", "tp", None),
        P("ep", "tp", None),
        P("ep", "tp", None),
        P("ep", "tp"),
        P("tp", None),
        P(("ep", "tp"), None),
        P(),
        P("ep", None, "tp"),
        P("ep", None, "tp"),
        P("ep", "tp", None),
        P(("ep", "tp"), None),
        P(("ep", "tp"), None),
    )
    out_specs = (P(("ep", "tp"), None), P(("ep", "tp"), None))
    return jax.shard_map(body, mesh=mesh, in_specs=in_specs, out_specs=out_specs, check_vma=False)
```

profile of v0, /device:TPU:8, one launch (start us, length us, event | category | flops | bytes accessed | tf_op | source)
XLA Modules:
  0.0 583.5 jit_solution(1064137814376958959)
XLA Ops:
  15.4 4.1 scatter_custom_fusion
  19.5 3.7 reshape.326
  23.2 63.4 %all_to_all.15 = bf16[64,6,2048]{2,1,0:T(8,128)(2,1)} all-to-all(bf16[64,6,2048]{2,1,0:T(8,128)(2,1)} %reshape.326), channel_id=1, replica_groups=mesh['ep'=64,'tp'=4] {'ep'}, dimensions={0} | all-to-all | bytes 3145728 | tf_op jit(solution)/shard_map/all_to_all | solution.py:157
  86.7 3.8 reshape.327
  93.4 3.7 collective-permute-done.1
  99.2 3.7 collective-permute-done.2
  103.5 3.6 collective-permute-done.3
  107.3 5.1 collective-permute-done.4
  113.9 41.0 %all-gather.5.cloned.1.call-done = bf16[1536,2048]{1,0:T(8,128)(2,1)} async-done(((bf16[384,2048]{1,0:T(8,128)(2,1)}), bf16[1536,2048]{1,0:T(8,128)(2,1)}) %all-gather.5.cloned.1.call-update) | async-done | bytes 6291472 | tf_op jit(solution)/shard_map/all_gather | solution.py:159
  155.0 8.6 %fusion.53 = f32[1536,512]{1,0:T(8,128)} fusion(bf16[1536,2048]{1,0:T(8,128)(2,1)} %all-gather.5.cloned.1.call-done, bf16[1,2048,512]{2,1,0:T(8,128)(2,1)} %param.23), kind=kOutput, calls=%fused_computation.82 | convolution fusion | flops 3221225472 | bytes 11534336 | tf_op jit(solution)/shard_map/dot_general | solution.py:46
  163.6 11.8 %convolution_convert_fusion = bf16[1536,2048]{1,0:T(8,128)(2,1)} fusion(bf16[1,512,2048]{2,1,0:T(8,128)(2,1)S(1)} %copy-done, bf16[1536,2048]{1,0:T(8,128)(2,1)} %all-gather.5.cloned.1.call-done, f32[1536,512]{1,0:T(8,128)} %fusion.53, bf16[1,2048,512]{2,1,0:T(8,128)(2,1)} %param.24), kind=kOutput, calls=%fused_computation.74 | convolution fusion | flops 6450315264 | bytes 19922944 | tf_op jit(solution)/shard_map/dot_general | solution.py:170
  175.3 5.3 all-to-all-start.1
  180.6 66.6 %all-gather.3.cloned.1.call-done = bf16[16384,258]{1,0:T(8,128)(2,1)} async-done(((bf16[256,258]{1,0:T(8,128)(2,1)}), bf16[16384,258]{1,0:T(8,128)(2,1)}) %all-gather.3.cloned.1.call-update) | async-done | bytes 8454160 | tf_op jit(solution)/shard_map/all_gather | solution.py:11
  247.2 5.7 slice_bitcast_fusion.4
  252.9 3.8 slice.59
  256.7 3.7 copy.53
  260.5 125.5 %while.31 = (s32[]{:T(128)}, f32[1,2,128,128]{3,2,1,0:T(8,128)S(1)}, f32[1,2,128]{2,1,0:T(2,128)S(1)}, s32[]{:T(128)}, s32[]{:T(128)}, /*index=5*/bf16[16384,1,1...) while((s32[]{:T(128)}, ...), condition=%wide.region_9.10_spmd.clone, body=%wide.region_5.9_spmd.clone.sunk | while | flops 176343936 | bytes 10775775 | solution.py:94
  278.4 2.5 fusion.100
  301.9 2.5 fusion.100
  325.4 2.5 fusion.100
  391.9 5.8 collective-permute-done.8
  397.7 4.3 collective-permute-done.9
  402.0 5.3 collective-permute-done.10
  407.3 4.2 reduce_sum.69
  413.1 10.0 %all-to-all-start.2 = ((bf16[64,6,2048]{2,1,0:T(8,128)(2,1)}), bf16[64,6,2048]{2,1,0:T(8,128)(2,1)}, u32[]{:S(2)}, u32[]{:S(2)}) async-start(bf16[64,6,2048]{2,1,0:T(8,128)(2,1)} %reshape.329), calls=%async_computation.3 | async-start | bytes 4194304 | tf_op jit(solution)/shard_map/all_to_all | solution.py:172
  423.2 8.1 %while.30 = (s32[]{:T(128)}, f32[1,2,128,128]{3,2,1,0:T(8,128)S(1)}, f32[1,2,128]{2,1,0:T(2,128)S(1)}, s32[]{:T(128)}, s32[]{:T(128)}, /*index=5*/bf16[16384,1,1...) while((s32[]{:T(128)}, ...), condition=%wide.region_4.5_spmd.clone, body=%wide.region_0.4_spmd.clone.sunk | while | flops 176343936 | bytes 10775775 | solution.py:94
  431.4 2.7 convolution_convert_fusion.1
  434.6 39.7 %all-to-all-done.2 = bf16[64,6,2048]{2,1,0:T(8,128)(2,1)} async-done(((bf16[64,6,2048]{2,1,0:T(8,128)(2,1)}), bf16[64,6,2048]{2,1,0:T(8,128)(2,1)}, u32[]{:S(2)}, u32[]{:S(2)}) %all-to-all-start.2) | async-done | bytes 1572896 | tf_op jit(solution)/shard_map/all_to_all | solution.py:172
  474.3 3.7 reshape.330
  478.0 4.1 gather_fusion
  483.6 6.2 %multiply_reduce_fusion = bf16[128,2048]{1,0:T(8,128)(2,1)} fusion(bf16[128,2,2048]{2,1,0:T(2,128)(2,1)} %gather.7, pred[128,2]{1,0:T(8,128)(4,1)S(1)} %copy.62, f32[128,2]{1,0:T(8,128)S(1)} %copy.64), kind=kLoop, calls=%fused_computation.84 | loop fusion | flops 1835008 | bytes 1574144 | tf_op jit(solution)/shard_map/reduce_sum | solution.py:183
  489.9 86.8 %reduce-scatter.2.cloned.1.call-done = bf16[64,2048]{1,0:T(8,128)(2,1)} async-done(((bf16[256,2048]{1,0:T(8,128)(2,1)}), bf16[64,2048]{1,0:T(8,128)(2,1)}) %reduce-scatter.2.cloned.1.call-update) | async-done | bytes 262160 | tf_op jit(solution)/shard_map/reduce_scatter | solution.py:163
  (296 shorter events, 149.3 us)
Async XLA Ops:
  7.2 156.4 %copy-start = (bf16[1,512,2048]{2,1,0:T(8,128)(2,1)S(1)}, bf16[1,512,2048]{2,1,0:T(8,128)(2,1)}, u32[]{:S(2)}) copy-start(bf16[1,512,2048]{2,1,0:T(8,128)(2,1)} %param.25) | copy-start | bytes 6291460
  7.2 147.8 %all-gather.5.cloned.1.call-start = ((), (), s32[]{:S(2)}) async-start(), calls=%async_computation.6 | async-start | bytes 7864320 | tf_op jit(solution)/shard_map/all_gather | solution.py:159
  86.6 3.8 copy-start.6
  86.7 4.0 copy-start.3
  86.7 4.0 copy-start.4
  86.7 4.7 copy-start.2
  90.4 156.8 %all-gather.3.cloned.1.call-start = ((), (), s32[]{:S(2)}) async-start(), calls=%async_computation.4 | async-start | bytes 12779520 | tf_op jit(solution)/shard_map/all_gather | solution.py:11
  91.5 1.3 collective-permute-start
  92.9 4.3 collective-permute-start.1
  97.1 5.8 collective-permute-start.2
  102.9 4.3 collective-permute-start.3
  107.2 5.2 collective-permute-start.4
  112.4 148.1 %collective-permute-start.5 = (bf16[128,2,128]{2,0,1:T(8,128)(2,1)S(1)}, bf16[128,2,128]{2,0,1:T(8,128)(2,1)S(1)}, u32[]{:S(2)}, u32[]{:S(2)}) collective-permute-start(bf16[128,2,128]{2,0,1:T(8,128)(2,1)S(1)} %collective-permute-done.4), channel_id=1, source_target_pairs={{0,128},{4,132},{8,136},{12,140},{16,144},{20,148},{24,152},{28,15... | collective-permute-start | bytes 196616 | tf_op jit(solution)/shard_map/ppermute | solution.py:22
  175.3 232.0 %all-to-all-start.1 = ((bf16[4,384,2048]{2,1,0:T(8,128)(2,1)}), bf16[4,384,2048]{2,1,0:T(8,128)(2,1)}, u32[]{:S(2)}, u32[]{:S(2)}) async-start(bf16[4,384,2048]{2,1,0:T(8,128)(2,1)} %bitcast.212), calls=%async_computation.2 | async-start | bytes 12582912 | tf_op jit(solution)/shard_map/all_to_all | solution.py:32
  386.1 1.3 collective-permute-start.6
  387.5 4.5 collective-permute-start.7
  391.9 5.8 collective-permute-start.8
  397.7 4.3 collective-permute-start.9
  402.0 5.3 collective-permute-start.10
  407.3 24.1 %collective-permute-start.11 = (bf16[128,256]{0,1:T(8,128)(2,1)S(1)}, bf16[128,256]{0,1:T(8,128)(2,1)S(1)}, u32[]{:S(2)}, u32[]{:S(2)}) collective-permute-start(bf16[128,256]{0,1:T(8,128)(2,1)S(1)} %collective-permute-done.10), channel_id=1, source_target_pairs={{0,128},{4,132},{8,136},{12,140},{16,144},{20,148},{24,152},{28,15... | collective-permute-start | bytes 196616 | tf_op jit(solution)/shard_map/ppermute | solution.py:22
  413.1 61.2 %all-to-all-start.2 = ((bf16[64,6,2048]{2,1,0:T(8,128)(2,1)}), bf16[64,6,2048]{2,1,0:T(8,128)(2,1)}, u32[]{:S(2)}, u32[]{:S(2)}) async-start(bf16[64,6,2048]{2,1,0:T(8,128)(2,1)} %reshape.329), calls=%async_computation.3 | async-start | bytes 4194304 | tf_op jit(solution)/shard_map/all_to_all | solution.py:172
  423.1 153.6 %reduce-scatter.2.cloned.1.call-start = ((), (), s32[]{:S(2)}) async-start(), calls=%async_computation.5 | async-start | bytes 1310720 | tf_op jit(solution)/shard_map/reduce_scatter | solution.py:163
  431.3 3.0 copy-start.5
  431.3 3.2 copy-start.7
  478.0 98.7 %copy-start.1 = (bf16[1,512,2048]{2,1,0:T(8,128)(2,1)S(1)}, bf16[1,512,2048]{2,1,0:T(8,128)(2,1)}, u32[]{:S(2)}) copy-start(bf16[1,512,2048]{2,1,0:T(8,128)(2,1)} %param.25) | copy-start | bytes 6291460
Sparse Core Ops, SparseCore 0:
  90.6 64.3 all-gather.4
  158.3 88.9 all-gather.2
  434.2 142.4 reduce-scatter.1
where the time goes:
time: 592 us; the launch traced here: 583 us
  waiting for transfers between devices  270 us (46%)
  other arithmetic  89.5 us (15%)
  matrix products  77.4 us (13%)
  blocking collectives  63.4 us (11%)
  local copies, waits for them, and re-layouts  43.9 us (7%)
  starting transfers between devices  22.8 us (4%)
  between operations  14.2 us (2%)
    reduce_scatter x1, waiting for transfers between devices, body(): lax.psum_scatter(jnp.dot(attended, out_weight, preferred_element_type=jnp...  86.8 us
    all_gather x1, waiting for transfers between devices, in_one_piece(): filled, at, done = (lax.all_gather(both, axis, axis=dim, tiled=True), 0, [])  66.6 us
    all_to_all x1, blocking collectives, body(): lax.all_to_all(outbound, 'ep', split_axis=0, concat_axis=0, tiled=True)  63.4 us
    another operation x36, other arithmetic  44.3 us
    all_gather x1, waiting for transfers between devices, body(): lax.all_gather(arrived.reshape(ep_count * capacity, model_width), 'tp', a...  41 us
    all_to_all x1, waiting for transfers between devices, body(): lax.all_to_all(expert_sum.astype(jnp.bfloat16).reshape(ep_count, capacity...  39.7 us
    ppermute x12, waiting for transfers between devices, partner(): return lax.ppermute(value, axis, pairs)  36.2 us
    dot_general x17, matrix products, visit(): jnp.einsum('rkgd,skd->kgrs', query_rows, key_tile_rows, preferred_element...  32.2 us
  transfers between devices with their start and end apart: 17, of which 14 were waited for; matrix products, arithmetic and copies ran while one was open for 33% of the time, Pallas kernels for 0%

commit v1 on v0

--- a/solution.py
+++ b/solution.py
@@ -1,8 +1,18 @@
+import functools
 import math
 import jax
 import jax.numpy as jnp
 from jax import lax
 from jax.sharding import PartitionSpec as P
+
+
+def targets_put(tile_in, ax_name):
+    clean = jnp.concatenate([tile_in for _ in range(jax.lax.psum(1, ax_name))], 0)
+    odd = jax.lax.all_to_all(clean, ax_name, 0, 0, tiled=True)
+    return odd
+
+
+point_tables = functools.partial(targets_put, ax_name="tp")
 
 
 def in_one_piece(arrays, axis, dim, along):
@@ -156,9 +166,7 @@
     down_rows = down_weight[0]
     arrived = lax.all_to_all(outbound, "ep", split_axis=0, concat_axis=0, tiled=True)
     hidden = swiglu_rows(
-        lax.all_gather(arrived.reshape(ep_count * capacity, model_width), "tp", axis=0, tiled=True),
-        gate_cols,
-        up_cols,
+        point_tables(arrived.reshape(ep_count * capacity, model_width)), gate_cols, up_cols
     )
     mixed_sum = lax.psum_scatter(
         jnp.dot(attended, out_weight, preferred_element_type=jnp.float32).astype(jnp.bfloat16),

time: 592 us -> 554 us (0.936)
  waiting for transfers between devices: 270 us -> 209 us
  blocking collectives: 63.4 us -> 76 us
  other arithmetic: 89.5 us -> 96.5 us
    all_gather x1, waiting for transfers between devices: 66.6 us -> 0.02 us  [in_one_piece(): filled, at, done = (lax.all_gather(both, axis, axis=dim, tiled=True), 0, [])]
    all_to_all x0 -> x1, waiting for transfers between devices: none -> 49.2 us  [targets_put(): odd = jax.lax.all_to_all(clean, ax_name, 0, 0, tiled=True)]
    all_gather x1 -> x0, waiting for transfers between devices: 41 us -> none  [body(): lax.all_gather(arrived.reshape(ep_count * capacity, model_width), 'tp', a...]
    all_to_all x1, waiting for transfers between devices: 39.7 us -> 0.01 us  [body(): lax.all_to_all(expert_sum.astype(jnp.bfloat16).reshape(ep_count, capacity...]
    ppermute x12, waiting for transfers between devices: 36.2 us -> 75.2 us  [partner(): return lax.ppermute(value, axis, pairs)]
    all_to_all x1, blocking collectives: 63.4 us -> 76 us  [body(): lax.all_to_all(outbound, 'ep', split_axis=0, concat_axis=0, tiled=True)]
    concatenate x0 -> x1, other arithmetic: none -> 6.15 us  [targets_put(): jnp.concatenate([tile_in for _ in range(jax.lax.psum(1, ax_name))], 0)]
  transfers between devices with their start and end apart: 17 -> 17, of which waited for: 14 -> 12; matrix products, arithmetic and copies ran while one was open for 33% -> 40% of each run, Pallas kernels for 0% -> 0%
where the time goes in v1:
time: 554 us; the launch traced here: 545 us
  waiting for transfers between devices  209 us (38%)
  other arithmetic  96.5 us (17%)
  matrix products  77.3 us (14%)
  blocking collectives  76 us (14%)
  local copies, waits for them, and re-layouts  44.6 us (8%)
  starting transfers between devices  24.9 us (4%)
  between operations  14.6 us (3%)
    reduce_scatter x1, waiting for transfers between devices, body(): lax.psum_scatter(jnp.dot(attended, out_weight, preferred_element_type=jnp...  84.5 us
    all_to_all x1, blocking collectives, body(): lax.all_to_all(outbound, 'ep', split_axis=0, concat_axis=0, tiled=True)  76 us
    ppermute x12, waiting for transfers between devices, partner(): return lax.ppermute(value, axis, pairs)  75.2 us
    all_to_all x1, waiting for transfers between devices, targets_put(): odd = jax.lax.all_to_all(clean, ax_name, 0, 0, tiled=True)  49.2 us
    another operation x36, other arithmetic  44.3 us
    dot_general x17, matrix products, visit(): jnp.einsum('rkgd,skd->kgrs', query_rows, key_tile_rows, preferred_element...  32.2 us
    convert_element_type x17, other arithmetic, visit(): weights = jnp.where(earlier, jnp.exp(jax.nn.log_sigmoid(scores) + after +...  26.1 us
    dot_general x17, matrix products, visit(): jnp.einsum('kgrs,skd->kgrd', weights, value_block, preferred_element_type...  22.1 us
  transfers between devices with their start and end apart: 17, of which 12 were waited for; matrix products, arithmetic and copies ran while one was open for 40% of the time, Pallas kernels for 0%

profile of v1, /device:TPU:8, one launch (start us, length us, event | category | flops | bytes accessed | tf_op | source)
XLA Modules:
  0.0 544.8 jit_solution(1459594962895497969)
XLA Ops:
  17.8 4.1 scatter_custom_fusion
  22.0 3.7 reshape.328
  25.7 76.0 %all_to_all.27 = bf16[64,6,2048]{2,1,0:T(8,128)(2,1)} all-to-all(bf16[64,6,2048]{2,1,0:T(8,128)(2,1)} %reshape.328), channel_id=1, replica_groups=mesh['ep'=64,'tp'=4] {'ep'}, dimensions={0} | all-to-all | bytes 3145728 | tf_op jit(solution)/shard_map/all_to_all | solution.py:167
  101.7 3.7 reshape.329
  105.5 6.2 %pad_maximum_fusion = bf16[1536,2048]{1,0:T(8,128)(2,1)} fusion(bf16[384,2048]{1,0:T(8,128)(2,1)} %reshape.329), kind=kLoop, calls=%fused_computation.75 | loop fusion | flops 25165824 | bytes 7864320 | tf_op jit(solution)/shard_map/concatenate | solution.py:10
  111.6 5.4 all-to-all-start.1
  118.6 4.3 collective-permute-done.1
  124.2 4.5 collective-permute-done.2
  128.7 4.3 collective-permute-done.3
  132.9 5.3 collective-permute-done.4
  138.8 49.2 %all-to-all-done.1 = bf16[4,384,2048]{2,1,0:T(8,128)(2,1)} async-done(((bf16[4,384,2048]{2,1,0:T(8,128)(2,1)}), bf16[4,384,2048]{2,1,0:T(8,128)(2,1)}, u32[]{:S(2)}, u32[]{:S(2)}) %all-to-all-start.1) | async-done | bytes 6291488 | tf_op jit(solution)/shard_map/all_to_all | solution.py:11
  188.0 8.6 %fusion.53 = f32[1536,512]{1,0:T(8,128)} fusion(bf16[1536,2048]{1,0:T(8,128)(2,1)} %bitcast.14, bf16[1,2048,512]{2,1,0:T(8,128)(2,1)} %param.23), kind=kOutput, calls=%fused_computation.83 | convolution fusion | flops 3221225472 | bytes 11534336 | tf_op jit(solution)/shard_map/dot_general | solution.py:56
  196.6 11.8 %convolution_convert_fusion = bf16[1536,2048]{1,0:T(8,128)(2,1)} fusion(bf16[1,512,2048]{2,1,0:T(8,128)(2,1)S(1)} %copy-done, bf16[1536,2048]{1,0:T(8,128)(2,1)} %bitcast.14, f32[1536,512]{1,0:T(8,128)} %fusion.53, bf16[1,2048,512]{2,1,0:T(8,128)(2,1)} %param.24), kind=kOutput, calls=%fused_computation.74 | convolution fusion | flops 6450315264 | bytes 19922944 | tf_op jit(solution)/shard_map/dot_general | solution.py:178
  208.4 5.2 all-to-all-start.2
  213.6 5.7 %slice_bitcast_fusion.4 = (bf16[16384,1,128]{2,0,1:T(8,128)(2,1)}, bf16[16384,1,128]{2,0,1:T(8,128)(2,1)}) fusion(bf16[16384,258]{1,0:T(8,128)(2,1)} %all-gather.2.cloned.1.call-done), kind=kLoop, calls=%fused_computation.76 | loop fusion | bytes 16777216 | tf_op jit(solution)/shard_map/reshape | solution.py:24
  219.3 3.8 slice.59
  223.1 3.7 copy.53
  226.9 125.5 %while.31 = (s32[]{:T(128)}, f32[1,2,128,128]{3,2,1,0:T(8,128)S(1)}, f32[1,2,128]{2,1,0:T(2,128)S(1)}, s32[]{:T(128)}, s32[]{:T(128)}, /*index=5*/bf16[16384,1,1...) while((s32[]{:T(128)}, ...), condition=%wide.region_9.10_spmd.clone, body=%wide.region_5.9_spmd.clone.sunk | while | flops 176343936 | bytes 10775775 | solution.py:104
  236.9 2.5 fusion.100
  354.0 4.3 collective-permute-done.7
  358.3 5.8 %collective-permute-done.8 = bf16[128,256]{0,1:T(8,128)(2,1)S(1)} collective-permute-done((bf16[128,256]{0,1:T(8,128)(2,1)S(1)}, bf16[128,256]{0,1:T(8,128)(2,1)S(1)}, u32[]{:S(2)}, u32[]{:S(2)}) %collective-permute-start.8) | collective-permute-done | bytes 65568 | tf_op jit(solution)/shard_map/ppermute | solution.py:32
  364.1 4.3 collective-permute-done.9
  368.4 4.2 reduce_sum.69
  374.1 6.4 %all-to-all-start.3 = ((bf16[64,6,2048]{2,1,0:T(8,128)(2,1)}), bf16[64,6,2048]{2,1,0:T(8,128)(2,1)}, u32[]{:S(2)}, u32[]{:S(2)}) async-start(bf16[64,6,2048]{2,1,0:T(8,128)(2,1)} %reshape.331), calls=%async_computation.4 | async-start | bytes 4194304 | tf_op jit(solution)/shard_map/all_to_all | solution.py:180
  380.6 5.6 %collective-permute-start.11 = (bf16[128,256]{0,1:T(8,128)(2,1)S(1)}, bf16[128,256]{0,1:T(8,128)(2,1)S(1)}, u32[]{:S(2)}, u32[]{:S(2)}) collective-permute-start(bf16[128,256]{0,1:T(8,128)(2,1)S(1)} %collective-permute-done.10), channel_id=1, source_target_pairs={{0,128},{4,132},{8,136},{12,140},{16,144},{20,148},{24,152},{28,15... | collective-permute-start | bytes 196616 | tf_op jit(solution)/shard_map/ppermute | solution.py:32
  386.2 8.1 %while.30 = (s32[]{:T(128)}, f32[1,2,128,128]{3,2,1,0:T(8,128)S(1)}, f32[1,2,128]{2,1,0:T(2,128)S(1)}, s32[]{:T(128)}, s32[]{:T(128)}, /*index=5*/bf16[16384,1,1...) while((s32[]{:T(128)}, ...), condition=%wide.region_4.5_spmd.clone, body=%wide.region_0.4_spmd.clone.sunk | while | flops 176343936 | bytes 10775775 | solution.py:104
  394.4 40.0 %collective-permute-done.11 = bf16[128,256]{0,1:T(8,128)(2,1)S(1)} collective-permute-done((bf16[128,256]{0,1:T(8,128)(2,1)S(1)}, bf16[128,256]{0,1:T(8,128)(2,1)S(1)}, u32[]{:S(2)}, u32[]{:S(2)}) %collective-permute-start.11) | collective-permute-done | bytes 65568 | tf_op jit(solution)/shard_map/ppermute | solution.py:32
  434.4 2.7 convolution_convert_fusion.1
  437.6 3.7 reshape.332
  441.3 4.1 gather_fusion
  447.0 6.2 %multiply_reduce_fusion = bf16[128,2048]{1,0:T(8,128)(2,1)} fusion(bf16[128,2,2048]{2,1,0:T(2,128)(2,1)} %gather.7, pred[128,2]{1,0:T(8,128)(4,1)S(1)} %copy.62, f32[128,2]{1,0:T(8,128)S(1)} %copy.64), kind=kLoop, calls=%fused_computation.85 | loop fusion | flops 1835008 | bytes 1574144 | tf_op jit(solution)/shard_map/reduce_sum | solution.py:191
  453.2 84.5 %reduce-scatter.2.cloned.1.call-done = bf16[64,2048]{1,0:T(8,128)(2,1)} async-done(((bf16[256,2048]{1,0:T(8,128)(2,1)}), bf16[64,2048]{1,0:T(8,128)(2,1)}) %reduce-scatter.2.cloned.1.call-update) | async-done | bytes 262160 | tf_op jit(solution)/shard_map/reduce_scatter | solution.py:171
  (290 shorter events, 148.6 us)
Async XLA Ops:
  7.2 189.4 %copy-start = (bf16[1,512,2048]{2,1,0:T(8,128)(2,1)S(1)}, bf16[1,512,2048]{2,1,0:T(8,128)(2,1)}, u32[]{:S(2)}) copy-start(bf16[1,512,2048]{2,1,0:T(8,128)(2,1)} %param.25) | copy-start | bytes 6291460
  7.2 206.5 %all-gather.2.cloned.1.call-start = ((), (), s32[]{:S(2)}) async-start(), calls=%async_computation.5 | async-start | bytes 12779520 | tf_op jit(solution)/shard_map/all_gather | solution.py:21
  111.6 5.4 copy-start.2
  111.6 76.4 %all-to-all-start.1 = ((bf16[4,384,2048]{2,1,0:T(8,128)(2,1)}), bf16[4,384,2048]{2,1,0:T(8,128)(2,1)}, u32[]{:S(2)}, u32[]{:S(2)}) async-start(bf16[4,384,2048]{2,1,0:T(8,128)(2,1)} %bitcast.214), calls=%async_computation.2 | async-start | bytes 12582912 | tf_op jit(solution)/shard_map/all_to_all | solution.py:11
  117.2 1.4 collective-permute-start
  118.6 4.3 collective-permute-start.1
  122.9 5.8 %collective-permute-start.2 = (bf16[128,2,128]{2,0,1:T(8,128)(2,1)S(1)}, bf16[128,2,128]{2,0,1:T(8,128)(2,1)S(1)}, u32[]{:S(2)}, u32[]{:S(2)}) collective-permute-start(bf16[128,2,128]{2,0,1:T(8,128)(2,1)S(1)} %collective-permute-done.1), channel_id=1, source_target_pairs={{0,16},{4,20},{8,24},{12,28},{16,0},{20,4},{24,8},{28,12},{32,48},... | collective-permute-start | bytes 196616 | tf_op jit(solution)/shard_map/ppermute | solution.py:32
  128.7 4.3 collective-permute-start.3
  132.9 5.3 collective-permute-start.4
  138.2 88.7 %collective-permute-start.5 = (bf16[128,2,128]{2,0,1:T(8,128)(2,1)S(1)}, bf16[128,2,128]{2,0,1:T(8,128)(2,1)S(1)}, u32[]{:S(2)}, u32[]{:S(2)}) collective-permute-start(bf16[128,2,128]{2,0,1:T(8,128)(2,1)S(1)} %collective-permute-done.4), channel_id=1, source_target_pairs={{0,128},{4,132},{8,136},{12,140},{16,144},{20,148},{24,152},{28,15... | collective-permute-start | bytes 196616 | tf_op jit(solution)/shard_map/ppermute | solution.py:32
  208.4 160.0 %all-to-all-start.2 = ((bf16[4,384,2048]{2,1,0:T(8,128)(2,1)}), bf16[4,384,2048]{2,1,0:T(8,128)(2,1)}, u32[]{:S(2)}, u32[]{:S(2)}) async-start(bf16[4,384,2048]{2,1,0:T(8,128)(2,1)} %bitcast.215), calls=%async_computation.3 | async-start | bytes 12582912 | tf_op jit(solution)/shard_map/all_to_all | solution.py:42
  352.5 1.3 collective-permute-start.6
  353.9 4.4 collective-permute-start.7
  358.3 5.8 %collective-permute-start.8 = (bf16[128,256]{0,1:T(8,128)(2,1)S(1)}, bf16[128,256]{0,1:T(8,128)(2,1)S(1)}, u32[]{:S(2)}, u32[]{:S(2)}) collective-permute-start(bf16[128,256]{0,1:T(8,128)(2,1)S(1)} %collective-permute-done.7), channel_id=1, source_target_pairs={{0,16},{4,20},{8,24},{12,28},{16,0},{20,4},{24,8},{28,12},{32,48},... | collective-permute-start | bytes 196616 | tf_op jit(solution)/shard_map/ppermute | solution.py:32
  364.1 4.3 collective-permute-start.9
  368.3 12.3 %collective-permute-start.10 = (bf16[128,256]{0,1:T(8,128)(2,1)S(1)}, bf16[128,256]{0,1:T(8,128)(2,1)S(1)}, u32[]{:S(2)}, u32[]{:S(2)}) collective-permute-start(bf16[128,256]{0,1:T(8,128)(2,1)S(1)} %collective-permute-done.9), channel_id=1, source_target_pairs={{0,64},{4,68},{8,72},{12,76},{16,80},{20,84},{24,88},{28,92},{32,9... | collective-permute-start | bytes 196616 | tf_op jit(solution)/shard_map/ppermute | solution.py:32
  374.1 63.5 %all-to-all-start.3 = ((bf16[64,6,2048]{2,1,0:T(8,128)(2,1)}), bf16[64,6,2048]{2,1,0:T(8,128)(2,1)}, u32[]{:S(2)}, u32[]{:S(2)}) async-start(bf16[64,6,2048]{2,1,0:T(8,128)(2,1)} %reshape.331), calls=%async_computation.4 | async-start | bytes 4194304 | tf_op jit(solution)/shard_map/all_to_all | solution.py:180
  380.5 157.2 %reduce-scatter.2.cloned.1.call-start = ((), (), s32[]{:S(2)}) async-start(), calls=%async_computation.6 | async-start | bytes 1310720 | tf_op jit(solution)/shard_map/reduce_scatter | solution.py:171
  380.6 53.8 %collective-permute-start.11 = (bf16[128,256]{0,1:T(8,128)(2,1)S(1)}, bf16[128,256]{0,1:T(8,128)(2,1)S(1)}, u32[]{:S(2)}, u32[]{:S(2)}) collective-permute-start(bf16[128,256]{0,1:T(8,128)(2,1)S(1)} %collective-permute-done.10), channel_id=1, source_target_pairs={{0,128},{4,132},{8,136},{12,140},{16,144},{20,148},{24,152},{28,15... | collective-permute-start | bytes 196616 | tf_op jit(solution)/shard_map/ppermute | solution.py:32
  394.3 43.0 %copy-start.3 = (s32[128,2]{0,1:T(2,128)S(1)}, s32[128,2]{0,1:T(2,128)}, u32[]{:S(2)}) copy-start(s32[128,2]{0,1:T(2,128)} %param.26) | copy-start | bytes 3076
  394.3 43.2 %copy-start.4 = (f32[128,2]{0,1:T(2,128)S(1)}, f32[128,2]{0,1:T(2,128)}, u32[]{:S(2)}) copy-start(f32[128,2]{0,1:T(2,128)} %param.27) | copy-start | bytes 3076
  441.3 96.4 %copy-start.1 = (bf16[1,512,2048]{2,1,0:T(8,128)(2,1)S(1)}, bf16[1,512,2048]{2,1,0:T(8,128)(2,1)}, u32[]{:S(2)}) copy-start(bf16[1,512,2048]{2,1,0:T(8,128)(2,1)} %param.25) | copy-start | bytes 6291460
Sparse Core Ops, SparseCore 0:
  11.3 110.2 all-gather.1
  437.2 100.4 reduce-scatter.1
